TPU v7x, 32 devices: a whole 2x2x4 slice. The times are simulated.
32 devices in a mesh: dp: 4 (over y, x), kv: 4 (over z), tp: 2 (over core).
Axes of the slice: x: 2, y: 2, z: 4, core: 2. Of those that a mesh axis runs over, the one named last changes fastest.
Arguments:
- tokens: bfloat16 [2048, 2048], P('dp', 'kv'), may hold values from -70 to 70
- pre_gain: float32 [2048], replicated, may hold values from 0.1 to 1.9
- query_weight: bfloat16 [2048, 1024], P(None, 'tp'), may hold values from -0.125 to 0.125
- key_weight: bfloat16 [2048, 1024], P(None, 'tp'), may hold values from -0.125 to 0.125
- value_weight: bfloat16 [2048, 1024], P(None, 'tp'), may hold values from -0.125 to 0.125
- gate_weight: bfloat16 [2048, 1024], P(None, 'tp'), may hold values from -0.125 to 0.125
- beta_weight: bfloat16 [2048, 8], replicated, may hold values from -0.125 to 0.125
- decay_weight: bfloat16 [2048, 8], replicated, may hold values from -0.125 to 0.125
- decay_log: float32 [8], P('tp'), may hold values from -3 to 0.5
- head_gain: float32 [128], replicated, may hold values from 0.1 to 1.9
- out_weight: bfloat16 [1024, 2048], P('tp', 'kv'), may hold values from -1 to 1
- post_gain: float32 [2048], P(('kv', 'tp')), may hold values from 0.1 to 1.9
- saved_state: float32 [512, 8, 128, 128], P(('dp', 'kv'), 'tp'), may hold values from -4 to 4
- earlier_keys: bfloat16 [512, 4, 8, 128], P(('dp', 'kv'), None, 'tp'), may hold values from -6 to 6
- earlier_values: bfloat16 [512, 4, 8, 128], P(('dp', 'kv'), None, 'tp'), may hold values from -6 to 6
- earlier_rates: float32 [512, 4, 8], P(('dp', 'kv'), None, 'tp'), may hold values from 0.05 to 0.95
- earlier_decays: float32 [512, 4, 8], P(('dp', 'kv'), None, 'tp'), may hold values from -1.5 to -0.02
- accepted: int32 [512], P(('dp', 'kv')), may hold values from 0 to 4
Outputs:
- mixed: bfloat16 [2048, 2048], P('dp', ('kv', 'tp'))
- committed: float32 [512, 8, 128, 128], P(('dp', 'kv'), 'tp')
All inputs are finite; a program needn't handle non-finite values.
Results may differ from a plain program's by a relative error of at most 0.011.
Values may be sent and summed in bfloat16 or wider, within the bound.
A program may use at most 128 MiB of HBM per device.

v0:
```python
import functools

import jax
import jax.numpy as jnp
from jax import lax
from jax.experimental import pallas as pl
from jax.experimental.pallas import tpu as pltpu
from jax.sharding import PartitionSpec as P

F32 = jnp.float32
BF16 = jnp.bfloat16
EPS = 1e-06
MESH_IDS = pl.DeviceIdType.MESH
VMEM_BYTES = 60 * 1024 * 1024


def mm(a, b):
    return jnp.dot(a, b, preferred_element_type=F32)


def mm_nt(a, b):
    return lax.dot_general(a, b, (((1,), (1,)), ((), ())), preferred_element_type=F32)


def mm_tn(a, b):
    return lax.dot_general(a, b, (((0,), (0,)), ((), ())), preferred_element_type=F32)


def mm_exact(a, b):
    return jnp.dot(a, b, preferred_element_type=F32, precision=lax.Precision.HIGHEST)


def unit(values):
    return values * lax.rsqrt(jnp.sum(values * values, axis=-1, keepdims=True) + EPS)


def silu(values):
    return values / (1.0 + jnp.exp(-values))


def masks_of(rows, proposals):
    r = lax.broadcasted_iota(jnp.int32, (rows, rows), 0)
    c = lax.broadcasted_iota(jnp.int32, (rows, rows), 1)
    same = (r // proposals) == (c // proposals)
    return same, same & (c <= r), same & (c < r)


def per_sequence(operands, state_of, proposals, rows):
    size = operands[0].shape[1]
    group = 16
    seqs = group // proposals
    stack = group * len(operands)
    row = lax.broadcasted_iota(jnp.int32, (stack, size), 0)
    owner = (row % group) // proposals
    outs = [[] for _ in operands]
    for g in range(rows // group):
        x = jnp.concatenate([o[g * group:(g + 1) * group] for o in operands], axis=0)
        lhs = jnp.concatenate(
            [jnp.where(owner == s, x, 0.0).astype(BF16) for s in range(seqs)], axis=1
        )
        rhs = state_of(g * seqs, seqs).reshape(seqs * size, size).astype(BF16)
        y = mm(lhs, rhs)
        for i in range(len(operands)):
            outs[i].append(y[i * group:(i + 1) * group])
    return [jnp.concatenate(o, axis=0) for o in outs]


def solve(keys, values, recalled, rate, decay_pairs, gamma, strict):
    kb = keys.astype(BF16)
    low = (jnp.where(strict, decay_pairs * mm_nt(kb, kb), 0.0) * rate).astype(BF16)
    rhs = rate * (values - gamma * recalled)
    square = mm(low, low).astype(BF16)
    x = rhs + mm(square, rhs.astype(BF16))
    return x - mm(low, x.astype(BF16))


def commit_kernel(proposals, keys_ref, values_ref, rates_ref, decays_ref, accepted_ref, state_ref, out_ref):
    h = pl.program_id(0)
    rows, size = keys_ref.shape
    seqs = accepted_ref.shape[1]
    same, incl, strict = masks_of(rows, proposals)
    row = lax.broadcasted_iota(jnp.int32, (rows, seqs), 0)
    own = (row // proposals) == lax.broadcasted_iota(jnp.int32, (rows, seqs), 1)

    def line(ref, p):
        return jnp.where(accepted_ref[...] > p, ref[p, pl.ds(h, 1), :], 0.0)

    def column(lines):
        spread = jnp.zeros((rows, seqs), F32)
        for p in range(proposals):
            spread = jnp.where(own & (row % proposals == p), lines[p], spread)
        return jnp.sum(spread, axis=1, keepdims=True)

    rate = column([line(rates_ref, p) for p in range(proposals)])
    sums = [line(decays_ref, 0)]
    for p in range(1, proposals):
        sums.append(sums[-1] + line(decays_ref, p))
    g_col = column(sums)
    g_last = column([sums[-1]] * proposals)
    g_row = jnp.broadcast_to(g_col, (rows, rows)).T
    pairs = jnp.exp(jnp.where(incl, g_col - g_row, -1e30))
    keys = unit(keys_ref[...].astype(F32))
    (recalled,) = per_sequence(
        [keys], lambda s, n: state_ref[s:s + n, 0], proposals, rows
    )
    w = solve(keys, values_ref[...].astype(F32), recalled, rate, pairs, jnp.exp(g_col), strict)
    scaled_keys = (keys * jnp.exp(g_last - g_col)).astype(BF16)
    whole = jnp.broadcast_to(jnp.exp(g_last), (rows, size))
    group = 16
    seqs = group // proposals
    owner = lax.broadcasted_iota(jnp.int32, (group, size), 0) // proposals
    for g in range(rows // group):
        wg = w[g * group:(g + 1) * group]
        spread = jnp.concatenate(
            [jnp.where(owner == s, wg, 0.0).astype(BF16) for s in range(seqs)], axis=1
        )
        add = mm_tn(scaled_keys[g * group:(g + 1) * group], spread)
        for s in range(seqs):
            seq = g * seqs + s
            keep = whole[seq * proposals:seq * proposals + 1]
            out_ref[seq, 0] = keep * state_ref[seq, 0] + add[:, s * size:(s + 1) * size]


def layer_kernel(
    kv, tp, proposals, heads, model_width,
    tokens, gains, qw, kw, vw, gw, beta_t, decay_t, log_rate, head_gain, ow, post, state,
    out,
    tok, wv, sv, owv, acc, bacc, dacc, att, passed, part, give, take, sums, sumall,
    w_sem, s_sem, ow_sem, own_sem, tok_send, tok_recv, half_send, half_recv, att_send, att_recv,
    tp_send, tp_recv, sum_send, sum_recv,
):
    me = lax.axis_index("kv")
    core = lax.axis_index("tp")
    rows, chunk = tok.shape[1], tok.shape[2]
    size = head_gain.shape[1]
    cols = out.shape[1]
    weights = (qw, kw, vw, gw)

    def source(d):
        return lax.rem(me - d + kv, kv)

    def target(d):
        return lax.rem(me + d, kv)

    local = {}
    local["tok"] = pltpu.make_async_copy(tokens.at[pl.ds(me * rows, rows), :], tok.at[0], own_sem)
    local["tok"].start()
    for d in range(kv):
        for i in range(4):
            local["w", i, d] = pltpu.make_async_copy(
                weights[i].at[pl.ds(source(d) * chunk, chunk), :], wv.at[i, d], w_sem.at[i, d]
            )
            local["w", i, d].start()
    for h in range(heads):
        local["s", h] = pltpu.make_async_copy(state.at[:, h], sv.at[h], s_sem.at[h])
        local["s", h].start()
    for o in range(tp):
        half = lax.rem(core + o, tp)
        if len(ow.shape) == 3:
            src = ow.at[half]
        else:
            src = ow.at[:, pl.ds(pl.multiple_of(half * cols, 128), cols)]
        local["o", o] = pltpu.make_async_copy(src, owv.at[o], ow_sem.at[o])
        local["o", o].start()

    barrier = pltpu.get_barrier_semaphore()
    group = kv * tp
    flat = me * tp + core

    def peer(o):
        other = lax.rem(flat + o, group)
        return {"kv": other // tp, "tp": lax.rem(other, tp)}

    for o in range(1, group):
        pl.semaphore_signal(barrier, inc=1, device_id=peer(o), device_id_type=MESH_IDS)
    pl.semaphore_wait(barrier, group - 1)

    part_rows = rows // tp
    mine_rows = pl.ds(pl.multiple_of(core * part_rows, part_rows), part_rows)
    sent = {}
    halves = {}
    for d in range(1, kv):
        sent[d] = pltpu.make_async_remote_copy(
            src_ref=tokens.at[
                pl.ds(pl.multiple_of(target(d) * rows + core * part_rows, part_rows), part_rows), :
            ],
            dst_ref=tok.at[d, mine_rows],
            send_sem=tok_send.at[d],
            recv_sem=tok_recv.at[d],
            device_id={"kv": target(d)},
            device_id_type=MESH_IDS,
        )
        sent[d].start()

    def hand_over(d):
        sent[d].wait_recv()
        for o in range(1, tp):
            halves[d, o] = pltpu.make_async_remote_copy(
                src_ref=tok.at[d, mine_rows],
                dst_ref=tok.at[d, mine_rows],
                send_sem=half_send.at[d, o],
                recv_sem=half_recv.at[d, o],
                device_id={"tp": lax.rem(core + o, tp)},
                device_id_type=MESH_IDS,
            )
            halves[d, o].start()

    def project(d, squares):
        if d == 0:
            local["tok"].wait()
        else:
            for o in range(1, tp):
                halves[d, o].wait_recv()
        c = source(d)
        span = pl.ds(pl.multiple_of(c * chunk, 128), chunk)
        wide = tok[d].astype(F32)
        scaled = (wide * gains[:, span]).astype(BF16)
        small_b = mm_nt(scaled, beta_t[:, span])
        small_d = mm_nt(scaled, decay_t[:, span])
        if d == 0:
            bacc[...] = small_b
            dacc[...] = small_d
        else:
            bacc[...] += small_b
            dacc[...] += small_d
        for i in range(4):
            local["w", i, d].wait()
            y = mm(scaled, wv[i, d])
            if d == 0:
                acc[i] = y
            else:
                acc[i] += y
        return squares + jnp.sum(wide * wide, axis=1, keepdims=True)

    squares = project(0, jnp.zeros((rows, 1), F32))
    for d in range(1, kv):
        hand_over(d)
        if d > 1:
            squares = project(d - 1, squares)
    if kv > 1:
        squares = project(kv - 1, squares)
    inverse = lax.rsqrt(squares / model_width + EPS)

    same, incl, strict = masks_of(rows, proposals)
    head_lane = lax.broadcasted_iota(jnp.int32, bacc.shape, 1)

    def column(values, h):
        return jnp.sum(jnp.where(head_lane == core * heads + h, values, 0.0), axis=1, keepdims=True)

    rates = 1.0 / (1.0 + jnp.exp(-bacc[...] * inverse))
    raw = dacc[...] * inverse
    soft = jnp.maximum(raw, 0.0) + jnp.log1p(jnp.exp(-jnp.abs(raw)))
    lane = lax.broadcasted_iota(jnp.int32, (rows, rows), 1)
    decays = jnp.zeros((rows, rows), F32)
    for h in range(heads):
        decay = -jnp.exp(jnp.full((rows, 1), log_rate[h], F32)) * column(soft, h)
        decays = jnp.where(lane == h, decay, decays)
    cum = mm_exact(jnp.where(incl, 1.0, 0.0), decays)
    cum_t = cum.T

    def hop(way, s, h):
        step = 1 if way == 0 else kv - 1
        return pltpu.make_async_remote_copy(
            src_ref=att.at[h] if s == 0 else passed.at[way, s, h],
            dst_ref=passed.at[way, s + 1, h],
            send_sem=att_send.at[way, s, h],
            recv_sem=att_recv.at[way, s + 1, h],
            device_id={"kv": lax.rem(me + step, kv)},
            device_id_type=MESH_IDS,
        )

    def arrives(way, s):
        return me - s >= 0 if way == 0 else me + s < kv

    def leaves(way):
        return me + 1 < kv if way == 0 else me >= 1

    def advance(turn):
        for s in range(kv):
            h = turn - s
            if not 0 <= h < heads:
                continue
            for way in range(2):
                if s == 0:
                    @pl.when(leaves(way))
                    def _():
                        hop(way, 0, h).start()
                else:
                    @pl.when(arrives(way, s))
                    def _():
                        hop(way, s - 1, h).wait_recv()
                    if s < kv - 1:
                        @pl.when(arrives(way, s) & leaves(way))
                        def _():
                            hop(way, s, h).start()

    def settle():
        for s in range(kv - 1):
            for way in range(2):
                @pl.when(arrives(way, s) & leaves(way))
                def _():
                    for h in range(heads):
                        hop(way, s, h).wait_send()

    for first in range(heads):
        batch = range(first, first + 1)
        local["s", first].wait()
        query, key, pairs, gamma, w, asked, reads = {}, {}, {}, {}, {}, {}, {}
        recalled = {}
        for h in batch:
            block = slice(h * size, (h + 1) * size)
            query[h] = unit(silu(acc[0, :, block] * inverse)) * size ** (-0.5)
            key[h] = unit(silu(acc[1, :, block] * inverse))
            pairs[h] = jnp.exp(jnp.where(incl, cum[:, h:h + 1] - cum_t[h:h + 1, :], -1e30))
            gamma[h] = jnp.exp(cum[:, h:h + 1])
        for h in batch:
            recalled[h], asked[h] = per_sequence(
                [key[h], query[h]], lambda s, n, h=h: sv[h, s:s + n], proposals, rows
            )
        for h in batch:
            value = silu(acc[2, :, h * size:(h + 1) * size] * inverse)
            w[h] = solve(key[h], value, recalled[h], column(rates, h), pairs[h], gamma[h], strict)
        for h in batch:
            mix = (pairs[h] * mm_nt(query[h].astype(BF16), key[h].astype(BF16))).astype(BF16)
            reads[h] = gamma[h] * asked[h] + mm(mix, w[h].astype(BF16))
        for h in batch:
            gate = silu(acc[3, :, h * size:(h + 1) * size] * inverse)
            scale = lax.rsqrt(jnp.mean(reads[h] * reads[h], axis=-1, keepdims=True) + EPS)
            att[h] = (reads[h] * scale * head_gain[...] * gate).astype(BF16)
        for h in batch:
            advance(h)

    for o in range(tp):
        local["o", o].wait()

    def swap(c, o):
        return pltpu.make_async_remote_copy(
            src_ref=give.at[c, o],
            dst_ref=take.at[c, o],
            send_sem=tp_send.at[c, o],
            recv_sem=tp_recv.at[c, o],
            device_id={"tp": lax.rem(core + o, tp)},
            device_id_type=MESH_IDS,
        )

    def combine(c, pieces):
        rows_in = jnp.concatenate(pieces, axis=1)
        for o in range(1, tp):
            give[c, o] = mm(rows_in, owv[o]).astype(BF16)
            swap(c, o).start()
        part[c] = mm(rows_in, owv[0])

    def finish(c):
        own = part[c]
        for o in range(1, tp):
            swap(c, o).wait_recv()
            own = own + take[c, o].astype(F32)
        part[c] = own
        total = jnp.sum(own * own, axis=1, keepdims=True)
        sums[pl.ds(c, 1), :] = jnp.broadcast_to(total, (rows, rows)).T[0:1]

    def blocks(turn):
        if turn < heads:
            return [(True, me, None)]
        s = turn - heads + 1
        return [(arrives(way, s), me - s if way == 0 else me + s, way) for way in range(2)]

    combine(me, [att[h] for h in range(heads)])
    for turn in range(heads, heads + kv - 1):
        advance(turn)
        s = turn - heads + 1
        for here, c, way in blocks(turn):
            @pl.when(here)
            def _():
                combine(c, [passed[way, s, h] for h in range(heads)])
        if s == 1:
            finish(me)
        else:
            for here, c, way in blocks(turn - 1):
                @pl.when(here)
                def _():
                    finish(c)
    if kv > 1:
        for here, c, way in blocks(heads + kv - 2):
            @pl.when(here)
            def _():
                finish(c)
    else:
        finish(me)
    tells = {}
    for o in range(1, group):
        tells[o] = pltpu.make_async_remote_copy(
            src_ref=sums,
            dst_ref=sumall.at[o],
            send_sem=sum_send.at[o],
            recv_sem=sum_recv.at[o],
            device_id=peer(o),
            device_id_type=MESH_IDS,
        )
        tells[o].start()
    settle()
    for d in range(1, kv):
        sent[d].wait_send()
        for o in range(1, tp):
            halves[d, o].wait_send()
    for c in range(kv):
        for o in range(1, tp):
            swap(c, o).wait_send()
    totals = sums[...]
    for o in range(1, group):
        tells[o].wait_recv()
        totals = totals + sumall[o]
    sums_factor = lax.rsqrt(totals / model_width + EPS)
    for o in range(1, group):
        tells[o].wait_send()
    for c in range(kv):
        factor = jnp.broadcast_to(sums_factor[c:c + 1, :], (rows, rows)).T[:, 0:1]
        out[c * rows:(c + 1) * rows, :] = (part[c] * factor * post[...]).astype(BF16)


def make_local(mesh):
    kv = mesh.shape["kv"]
    tp = mesh.shape["tp"]

    def local(
        tokens, pre_gain, query_weight, key_weight, value_weight, gate_weight, beta_weight,
        decay_weight, decay_log, head_gain, out_weight, post_gain, saved_state, earlier_keys,
        earlier_values, earlier_rates, earlier_decays, accepted,
    ):
        seqs, heads, size = saved_state.shape[:3]
        proposals = earlier_keys.shape[1]
        rows = seqs * proposals
        width = heads * size
        model_width = pre_gain.shape[0]
        chunk = tokens.shape[1]
        cols = post_gain.shape[0]
        state_spec = pl.BlockSpec((seqs, 1, size, size), lambda h: (0, h, 0, 0))
        row_spec = pl.BlockSpec((rows, size), lambda h: (0, h))
        scalar_spec = pl.BlockSpec((proposals, heads, seqs), lambda h: (0, 0, 0))
        committed = pl.pallas_call(
            functools.partial(commit_kernel, proposals),
            grid=(heads,),
            out_shape=jax.ShapeDtypeStruct(saved_state.shape, F32),
            in_specs=[
                row_spec, row_spec, scalar_spec, scalar_spec,
                pl.BlockSpec((1, seqs), lambda h: (0, 0)), state_spec,
            ],
            out_specs=state_spec,
            compiler_params=pltpu.CompilerParams(vmem_limit_bytes=VMEM_BYTES),
            cost_estimate=pl.CostEstimate(
                flops=2 * saved_state.size * 2 * proposals,
                bytes_accessed=saved_state.size * 8,
                transcendentals=0,
            ),
            name="commit",
        )(
            earlier_keys.reshape(rows, width),
            earlier_values.reshape(rows, width),
            jnp.transpose(earlier_rates, (1, 2, 0)),
            jnp.transpose(earlier_decays, (1, 2, 0)),
            accepted.reshape(1, seqs),
            saved_state,
        )

        if cols % 128:
            out_w = jnp.moveaxis(out_weight.reshape(width, tp, cols), 1, 0)
        else:
            out_w = out_weight
        any_spec = pl.BlockSpec(memory_space=pl.ANY)
        vmem_spec = pl.BlockSpec(memory_space=pltpu.VMEM)
        dma = pltpu.SemaphoreType.DMA
        mixed = pl.pallas_call(
            functools.partial(layer_kernel, kv, tp, proposals, heads, model_width),
            out_shape=jax.ShapeDtypeStruct((tokens.shape[0], cols), BF16),
            in_specs=[any_spec, vmem_spec] + [any_spec] * 4 + [vmem_spec] * 2
            + [pl.BlockSpec(memory_space=pltpu.SMEM), vmem_spec, any_spec, vmem_spec, any_spec],
            out_specs=vmem_spec,
            scratch_shapes=[
                pltpu.VMEM((kv, rows, chunk), BF16),
                pltpu.VMEM((4, kv, chunk, width), BF16),
                pltpu.VMEM((heads, seqs, size, size), F32),
                pltpu.VMEM((tp, width, cols), BF16),
                pltpu.VMEM((4, rows, width), F32),
                pltpu.VMEM((rows, heads * tp), F32),
                pltpu.VMEM((rows, heads * tp), F32),
                pltpu.VMEM((heads, rows, size), BF16),
                pltpu.VMEM((2, kv, heads, rows, size), BF16),
                pltpu.VMEM((kv, rows, cols), F32),
                pltpu.VMEM((kv, tp, rows, cols), BF16),
                pltpu.VMEM((kv, tp, rows, cols), BF16),
                pltpu.VMEM((kv, rows), F32),
                pltpu.VMEM((kv * tp, kv, rows), F32),
                dma((4, kv)), dma((heads,)), dma((tp,)), dma, dma((kv,)), dma((kv,)),
                dma((kv, tp)), dma((kv, tp)), dma((2, kv, heads)), dma((2, kv, heads)),
                dma((kv, tp)), dma((kv, tp)), dma((kv * tp,)), dma((kv * tp,)),
            ],
            compiler_params=pltpu.CompilerParams(
                collective_id=0, has_side_effects=True, vmem_limit_bytes=VMEM_BYTES
            ),
            name="layer",
        )(
            tokens, pre_gain.reshape(1, model_width), query_weight, key_weight, value_weight,
            gate_weight, beta_weight.T, decay_weight.T, decay_log, head_gain.reshape(1, size), out_w,
            post_gain.reshape(1, cols), committed,
        )
        return (mixed, committed)

    return local


def solution(mesh):
    placed = (
        P("dp", "kv"),
        P(),
        P(None, "tp"),
        P(None, "tp"),
        P(None, "tp"),
        P(None, "tp"),
        P(),
        P(),
        P("tp"),
        P(),
        P("tp", "kv"),
        P(("kv", "tp")),
        P(("dp", "kv"), "tp", None, None),
        P(("dp", "kv"), None, "tp", None),
        P(("dp", "kv"), None, "tp", None),
        P(("dp", "kv"), None, "tp"),
        P(("dp", "kv"), None, "tp"),
        P(("dp", "kv")),
    )
    return jax.shard_map(
        make_local(mesh),
        mesh=mesh,
        in_specs=placed,
        out_specs=(P("dp", ("kv", "tp")), P(("dp", "kv"), "tp", None, None)),
        check_vma=False,
    )
```

profile of v0, /device:TPU:0, one launch (start us, length us, event | category | flops | bytes accessed | tf_op | source)
XLA Modules:
  0.0 52.0 jit_solution(7719303605251391067)
XLA Ops:
  0.6 1.7 %copy_bitcast_fusion = (bf16[128,512]{1,0:T(8,128)(2,1)}, bf16[128,512]{1,0:T(8,128)(2,1)}) fusion(bf16[16,8,4,128]{3,2,1,0:T(4,128)(2,1)} %bitcast.16, bf16[16,8,4,128]{3,2,1,0:T(4,128)(2,1)} %bitcast.17), kind=kLoop, calls=%fused_computation | loop fusion | bytes 524288 | tf_op jit(solution)/shard_map/reshape | solution.py:458
  2.3 9.5 %commit.1.state = f32[32,4,128,128]{3,2,1,0:T(8,128)} custom-call(bf16[128,512]{1,0:T(8,128)(2,1)} %get-tuple-element.3.keys_ref, bf16[128,512]{1,0:T(8,128)(2,1)} %get-tuple-element.2.values_ref, f32[4,4,32]{2,1,0:T(4,128)} %bitcast.20, f32[4,4,32]{2,1,0:T(4,128)} %bitcast.21, s32[1,32]{1,0:T(1,128)} %bitcast.24, f32[32,4,128,128]{3,2,1,0:T(8,128)} %state_ref.1), custom_call_target="tpu_custom_call" | custom-call | flops 33554432 | bytes 16777216 | tf_op jit(solution)/shard_map/commit/pallas_call | solution.py:440
  11.8 38.6 %layer.1 = bf16[512,256]{1,0:T(8,128)(2,1)} custom-call(bf16[512,512]{1,0:T(8,128)(2,1)} %tokens.1, f32[1,2048]{1,0:T(1,128)} %bitcast.22, bf16[2048,512]{1,0:T(8,128)(2,1)} %qw.1, bf16[2048,512]{1,0:T(8,128)(2,1)} %kw.1, bf16[2048,512]{1,0:T(8,128)(2,1)} %vw.1, bf16[2048,512]{1,0:T(8,128)(2,1)} %gw.1, bf16[8,2048]{1,0:T(8,128)(2,1)} %bitcast.18, ...), custom_call_target="tpu_custom_call" | custom-call | tf_op jit(solution)/shard_map/layer/pallas_call | solution.py:472
  50.4 1.7 %copy.25 = bf16[512,256]{1,0:T(8,128)(2,1)} copy(bf16[512,256]{1,0:T(8,128)(2,1)} %layer.1) | data formatting | bytes 524288
where the time goes:
time: 52.3 us; the launch traced here: 52 us
  Pallas kernels  48 us (92%)
  local copies, waits for them, and re-layouts  3.36 us (6%)
  between operations  0.64 us (1%)
    pallas_call x1, Pallas kernels, local(): pl.pallas_call(functools.partial(layer_kernel, kv, tp, proposals, heads,...  38.6 us
    pallas_call x1, Pallas kernels, local(): pl.pallas_call(functools.partial(commit_kernel, proposals), grid=(heads,)...  9.46 us
    reshape x1, local copies, waits for them, and re-layouts, local(): earlier_values.reshape(rows, width)  1.69 us
    unnamed x1, local copies, waits for them, and re-layouts  1.67 us

commit v1 on v0

--- a/solution.py
+++ b/solution.py
@@ -11,7 +11,7 @@
 BF16 = jnp.bfloat16
 EPS = 1e-06
 MESH_IDS = pl.DeviceIdType.MESH
-VMEM_BYTES = 60 * 1024 * 1024
+VMEM_BYTES = 36 * 1024 * 1024
 
 
 def mm(a, b):
@@ -74,60 +74,91 @@
     return x - mm(low, x.astype(BF16))
 
 
-def commit_kernel(proposals, keys_ref, values_ref, rates_ref, decays_ref, accepted_ref, state_ref, out_ref):
-    h = pl.program_id(0)
-    rows, size = keys_ref.shape
-    seqs = accepted_ref.shape[1]
-    same, incl, strict = masks_of(rows, proposals)
-    row = lax.broadcasted_iota(jnp.int32, (rows, seqs), 0)
-    own = (row // proposals) == lax.broadcasted_iota(jnp.int32, (rows, seqs), 1)
-
-    def line(ref, p):
-        return jnp.where(accepted_ref[...] > p, ref[p, pl.ds(h, 1), :], 0.0)
-
-    def column(lines):
-        spread = jnp.zeros((rows, seqs), F32)
-        for p in range(proposals):
-            spread = jnp.where(own & (row % proposals == p), lines[p], spread)
-        return jnp.sum(spread, axis=1, keepdims=True)
-
-    rate = column([line(rates_ref, p) for p in range(proposals)])
-    sums = [line(decays_ref, 0)]
+def head_masks(rows, group, heads):
+    r = lax.broadcasted_iota(jnp.int32, (rows, rows), 0)
+    c = lax.broadcasted_iota(jnp.int32, (rows, rows), 1)
+    same = ((r // group) == (c // group)) & ((r % heads) == (c % heads))
+    return same & (c <= r), same & (c < r)
+
+
+def commit_table(proposals, heads, rates, decays, accepted):
+    seqs = accepted.shape[1]
+    live = [accepted > p for p in range(proposals)]
+    rate = jnp.concatenate([jnp.where(live[p], rates[p], 0.0) for p in range(proposals)], axis=0)
+    sums = [jnp.where(live[0], decays[0], 0.0)]
     for p in range(1, proposals):
-        sums.append(sums[-1] + line(decays_ref, p))
-    g_col = column(sums)
-    g_last = column([sums[-1]] * proposals)
+        sums.append(sums[-1] + jnp.where(live[p], decays[p], 0.0))
+    cum = jnp.concatenate(sums, axis=0)
+    last = jnp.concatenate([sums[-1]] * proposals, axis=0)
+    used = 3 * proposals * heads
+    table = jnp.concatenate([rate, cum, last], axis=0)
+    table = jnp.concatenate([table, jnp.zeros((used, 128 - seqs), F32)], axis=1)
+    table = jnp.concatenate([table, jnp.zeros((128 - used, 128), F32)], axis=0)
+    return table.T
+
+
+def commit_block(block, proposals, heads, table, keys_raw, values, masks, com, sbf):
+    rows, size = keys_raw.shape
+    group = proposals * heads
+    seqs = rows // group
+    incl, strict = masks
+    spread = jnp.concatenate(
+        [
+            jnp.broadcast_to(table[block * seqs + i:block * seqs + i + 1, :], (group, 128))
+            for i in range(seqs)
+        ],
+        axis=0,
+    )
+    lane = lax.broadcasted_iota(jnp.int32, (rows, 128), 1)
+    slot = lax.broadcasted_iota(jnp.int32, (rows, 128), 0) % group
+
+    def column(k):
+        return jnp.sum(jnp.where(lane == k * group + slot, spread, 0.0), axis=1, keepdims=True)
+
+    rate, g_col, g_last = column(0), column(1), column(2)
     g_row = jnp.broadcast_to(g_col, (rows, rows)).T
     pairs = jnp.exp(jnp.where(incl, g_col - g_row, -1e30))
-    keys = unit(keys_ref[...].astype(F32))
-    (recalled,) = per_sequence(
-        [keys], lambda s, n: state_ref[s:s + n, 0], proposals, rows
+    keys = unit(keys_raw.astype(F32))
+    owner = lax.broadcasted_iota(jnp.int32, (group, size), 0) % heads
+
+    def widen(x):
+        return jnp.concatenate(
+            [jnp.where(owner == h, x, 0.0).astype(BF16) for h in range(heads)], axis=1
+        )
+
+    recalled = jnp.concatenate(
+        [
+            mm(
+                widen(keys[i * group:(i + 1) * group]),
+                com[block * seqs + i].reshape(heads * size, size).astype(BF16),
+            )
+            for i in range(seqs)
+        ],
+        axis=0,
     )
-    w = solve(keys, values_ref[...].astype(F32), recalled, rate, pairs, jnp.exp(g_col), strict)
+    w = solve(keys, values.astype(F32), recalled, rate, pairs, jnp.exp(g_col), strict)
     scaled_keys = (keys * jnp.exp(g_last - g_col)).astype(BF16)
     whole = jnp.broadcast_to(jnp.exp(g_last), (rows, size))
-    group = 16
-    seqs = group // proposals
-    owner = lax.broadcasted_iota(jnp.int32, (group, size), 0) // proposals
-    for g in range(rows // group):
-        wg = w[g * group:(g + 1) * group]
-        spread = jnp.concatenate(
-            [jnp.where(owner == s, wg, 0.0).astype(BF16) for s in range(seqs)], axis=1
-        )
-        add = mm_tn(scaled_keys[g * group:(g + 1) * group], spread)
-        for s in range(seqs):
-            seq = g * seqs + s
-            keep = whole[seq * proposals:seq * proposals + 1]
-            out_ref[seq, 0] = keep * state_ref[seq, 0] + add[:, s * size:(s + 1) * size]
+    for i in range(seqs):
+        seq = block * seqs + i
+        span = slice(i * group, (i + 1) * group)
+        add = mm_tn(scaled_keys[span], widen(w[span]))
+        for h in range(heads):
+            keep = whole[i * group + h:i * group + h + 1]
+            new = keep * com[seq, h] + add[:, h * size:(h + 1) * size]
+            com[seq, h] = new
+            sbf[h, seq] = new.astype(BF16)
 
 
 def layer_kernel(
     kv, tp, proposals, heads, model_width,
-    tokens, gains, qw, kw, vw, gw, beta_t, decay_t, log_rate, head_gain, ow, post, state,
-    out,
-    tok, wv, sv, owv, acc, bacc, dacc, att, passed, part, give, take, sums, sumall,
-    w_sem, s_sem, ow_sem, own_sem, tok_send, tok_recv, half_send, half_recv, att_send, att_recv,
-    tp_send, tp_recv, sum_send, sum_recv,
+    tokens, gains_h, qw, kw, vw, gw, beta_h, decay_h, log_h, head_gain_h, ow, post_h, state,
+    ekeys_h, evalues_h, erates_h, edecays_h, accepted_h,
+    out, com,
+    tokv, tok, wv, sbf, owv, acc, sacc, att, passed, part, give, take, sums, sumall,
+    gains, beta_t, decay_t, log_rate, head_gain, post, ekeys, evalues, erates, edecays, accepted,
+    w_sem, s_sem, ow_sem, own_sem, small_sem, tok_send, tok_recv, half_send, half_recv,
+    att_send, att_recv, tp_send, tp_recv, sum_send, sum_recv,
 ):
     me = lax.axis_index("kv")
     core = lax.axis_index("tp")
@@ -142,18 +173,41 @@
     def target(d):
         return lax.rem(me + d, kv)
 
+    barrier = pltpu.get_barrier_semaphore()
+    group = kv * tp
+    flat = me * tp + core
+
+    def peer(o):
+        other = lax.rem(flat + o, group)
+        return {"kv": other // tp, "tp": lax.rem(other, tp)}
+
+    for o in range(1, group):
+        pl.semaphore_signal(barrier, inc=1, device_id=peer(o), device_id_type=MESH_IDS)
+
     local = {}
-    local["tok"] = pltpu.make_async_copy(tokens.at[pl.ds(me * rows, rows), :], tok.at[0], own_sem)
+    local["tok"] = pltpu.make_async_copy(tokens, tokv, own_sem)
     local["tok"].start()
+    pairs_small = (
+        (ekeys_h, ekeys), (evalues_h, evalues), (erates_h, erates), (edecays_h, edecays),
+        (accepted_h, accepted), (gains_h, gains), (beta_h, beta_t), (decay_h, decay_t),
+        (log_h, log_rate), (head_gain_h, head_gain), (post_h, post),
+    )
+    for i, (src, dst) in enumerate(pairs_small):
+        local["small", i] = pltpu.make_async_copy(src, dst, small_sem.at[i])
+        local["small", i].start()
+    block_rows = min(128, ekeys.shape[0])
+    blocks_n = ekeys.shape[0] // block_rows
+    block_seqs = state.shape[0] // blocks_n
+    for b in range(blocks_n):
+        span = pl.ds(b * block_seqs, block_seqs)
+        local["s", b] = pltpu.make_async_copy(state.at[span], com.at[span], s_sem.at[b])
+        local["s", b].start()
     for d in range(kv):
         for i in range(4):
             local["w", i, d] = pltpu.make_async_copy(
                 weights[i].at[pl.ds(source(d) * chunk, chunk), :], wv.at[i, d], w_sem.at[i, d]
             )
             local["w", i, d].start()
-    for h in range(heads):
-        local["s", h] = pltpu.make_async_copy(state.at[:, h], sv.at[h], s_sem.at[h])
-        local["s", h].start()
     for o in range(tp):
         half = lax.rem(core + o, tp)
         if len(ow.shape) == 3:
@@ -163,16 +217,7 @@
         local["o", o] = pltpu.make_async_copy(src, owv.at[o], ow_sem.at[o])
         local["o", o].start()
 
-    barrier = pltpu.get_barrier_semaphore()
-    group = kv * tp
-    flat = me * tp + core
-
-    def peer(o):
-        other = lax.rem(flat + o, group)
-        return {"kv": other // tp, "tp": lax.rem(other, tp)}
-
-    for o in range(1, group):
-        pl.semaphore_signal(barrier, inc=1, device_id=peer(o), device_id_type=MESH_IDS)
+    local["tok"].wait()
     pl.semaphore_wait(barrier, group - 1)
 
     part_rows = rows // tp
@@ -181,7 +226,7 @@
     halves = {}
     for d in range(1, kv):
         sent[d] = pltpu.make_async_remote_copy(
-            src_ref=tokens.at[
+            src_ref=tokv.at[
                 pl.ds(pl.multiple_of(target(d) * rows + core * part_rows, part_rows), part_rows), :
             ],
             dst_ref=tok.at[d, mine_rows],
@@ -206,23 +251,21 @@
             halves[d, o].start()
 
     def project(d, squares):
-        if d == 0:
-            local["tok"].wait()
-        else:
+        if d > 0:
             for o in range(1, tp):
                 halves[d, o].wait_recv()
         c = source(d)
         span = pl.ds(pl.multiple_of(c * chunk, 128), chunk)
-        wide = tok[d].astype(F32)
+        if d == 0:
+            wide = tokv[pl.ds(pl.multiple_of(me * rows, rows), rows), :].astype(F32)
+        else:
+            wide = tok[d].astype(F32)
         scaled = (wide * gains[:, span]).astype(BF16)
-        small_b = mm_nt(scaled, beta_t[:, span])
-        small_d = mm_nt(scaled, decay_t[:, span])
+        thin = mm_nt(scaled, jnp.concatenate([beta_t[:, span], decay_t[:, span]], axis=0))
         if d == 0:
-            bacc[...] = small_b
-            dacc[...] = small_d
+            sacc[...] = thin
         else:
-            bacc[...] += small_b
-            dacc[...] += small_d
+            sacc[...] += thin
         for i in range(4):
             local["w", i, d].wait()
             y = mm(scaled, wv[i, d])
@@ -232,30 +275,46 @@
                 acc[i] += y
         return squares + jnp.sum(wide * wide, axis=1, keepdims=True)
 
-    squares = project(0, jnp.zeros((rows, 1), F32))
-    for d in range(1, kv):
-        hand_over(d)
-        if d > 1:
-            squares = project(d - 1, squares)
-    if kv > 1:
-        squares = project(kv - 1, squares)
+    for i in range(len(pairs_small)):
+        local["small", i].wait()
+    table = commit_table(proposals, heads, erates[...], edecays[...], accepted[...])
+    commit_masks = head_masks(block_rows, proposals * heads, heads)
+    squares = jnp.zeros((rows, 1), F32)
+    steps = max(blocks_n, kv)
+    for b in range(steps):
+        if b < blocks_n:
+            span = slice(b * block_rows, (b + 1) * block_rows)
+            local["s", b].wait()
+            commit_block(
+                b, proposals, heads, table, ekeys[span], evalues[span], commit_masks, com, sbf
+            )
+        if 1 <= b < kv:
+            hand_over(b)
+        if b >= 1 and b - 1 < kv - 1:
+            squares = project(b - 1, squares)
+    squares = project(kv - 1, squares)
     inverse = lax.rsqrt(squares / model_width + EPS)
 
     same, incl, strict = masks_of(rows, proposals)
-    head_lane = lax.broadcasted_iota(jnp.int32, bacc.shape, 1)
-
-    def column(values, h):
-        return jnp.sum(jnp.where(head_lane == core * heads + h, values, 0.0), axis=1, keepdims=True)
-
-    rates = 1.0 / (1.0 + jnp.exp(-bacc[...] * inverse))
-    raw = dacc[...] * inverse
+    all_heads = heads * tp
+    pad = jnp.zeros((rows, 128 - 2 * all_heads), F32)
+    raw = jnp.concatenate([sacc[...] * inverse, pad], axis=1)
+    raw = pltpu.roll(raw, lax.rem(128 - core * heads, 128), axis=1)
+    rates = 1.0 / (1.0 + jnp.exp(-raw))
     soft = jnp.maximum(raw, 0.0) + jnp.log1p(jnp.exp(-jnp.abs(raw)))
-    lane = lax.broadcasted_iota(jnp.int32, (rows, rows), 1)
-    decays = jnp.zeros((rows, rows), F32)
-    for h in range(heads):
-        decay = -jnp.exp(jnp.full((rows, 1), log_rate[h], F32)) * column(soft, h)
-        decays = jnp.where(lane == h, decay, decays)
-    cum = mm_exact(jnp.where(incl, 1.0, 0.0), decays)
+    speed = jnp.concatenate(
+        [
+            jnp.zeros((1, all_heads), F32), jnp.exp(log_rate[...]),
+            jnp.zeros((1, 128 - all_heads - heads), F32),
+        ],
+        axis=1,
+    )
+    cum = -speed * soft
+    place = lax.broadcasted_iota(jnp.int32, (rows, 128), 0) % proposals
+    step = 1
+    while step < proposals:
+        cum = cum + jnp.where(place >= step, pltpu.roll(cum, step, axis=0), 0.0)
+        step *= 2
     cum_t = cum.T
 
     def hop(way, s, h):
@@ -304,22 +363,21 @@
 
     for first in range(heads):
         batch = range(first, first + 1)
-        local["s", first].wait()
         query, key, pairs, gamma, w, asked, reads = {}, {}, {}, {}, {}, {}, {}
         recalled = {}
         for h in batch:
             block = slice(h * size, (h + 1) * size)
             query[h] = unit(silu(acc[0, :, block] * inverse)) * size ** (-0.5)
             key[h] = unit(silu(acc[1, :, block] * inverse))
-            pairs[h] = jnp.exp(jnp.where(incl, cum[:, h:h + 1] - cum_t[h:h + 1, :], -1e30))
-            gamma[h] = jnp.exp(cum[:, h:h + 1])
+            pairs[h] = jnp.exp(jnp.where(incl, cum[:, all_heads + h:all_heads + h + 1] - cum_t[all_heads + h:all_heads + h + 1, :], -1e30))
+            gamma[h] = jnp.exp(cum[:, all_heads + h:all_heads + h + 1])
         for h in batch:
             recalled[h], asked[h] = per_sequence(
-                [key[h], query[h]], lambda s, n, h=h: sv[h, s:s + n], proposals, rows
+                [key[h], query[h]], lambda s, n, h=h: sbf[h, s:s + n], proposals, rows
             )
         for h in batch:
             value = silu(acc[2, :, h * size:(h + 1) * size] * inverse)
-            w[h] = solve(key[h], value, recalled[h], column(rates, h), pairs[h], gamma[h], strict)
+            w[h] = solve(key[h], value, recalled[h], rates[:, h:h + 1], pairs[h], gamma[h], strict)
         for h in batch:
             mix = (pairs[h] * mm_nt(query[h].astype(BF16), key[h].astype(BF16))).astype(BF16)
             reads[h] = gamma[h] * asked[h] + mm(mix, w[h].astype(BF16))
@@ -434,55 +492,31 @@
         model_width = pre_gain.shape[0]
         chunk = tokens.shape[1]
         cols = post_gain.shape[0]
-        state_spec = pl.BlockSpec((seqs, 1, size, size), lambda h: (0, h, 0, 0))
-        row_spec = pl.BlockSpec((rows, size), lambda h: (0, h))
-        scalar_spec = pl.BlockSpec((proposals, heads, seqs), lambda h: (0, 0, 0))
-        committed = pl.pallas_call(
-            functools.partial(commit_kernel, proposals),
-            grid=(heads,),
-            out_shape=jax.ShapeDtypeStruct(saved_state.shape, F32),
-            in_specs=[
-                row_spec, row_spec, scalar_spec, scalar_spec,
-                pl.BlockSpec((1, seqs), lambda h: (0, 0)), state_spec,
-            ],
-            out_specs=state_spec,
-            compiler_params=pltpu.CompilerParams(vmem_limit_bytes=VMEM_BYTES),
-            cost_estimate=pl.CostEstimate(
-                flops=2 * saved_state.size * 2 * proposals,
-                bytes_accessed=saved_state.size * 8,
-                transcendentals=0,
-            ),
-            name="commit",
-        )(
-            earlier_keys.reshape(rows, width),
-            earlier_values.reshape(rows, width),
-            jnp.transpose(earlier_rates, (1, 2, 0)),
-            jnp.transpose(earlier_decays, (1, 2, 0)),
-            accepted.reshape(1, seqs),
-            saved_state,
-        )
-
         if cols % 128:
             out_w = jnp.moveaxis(out_weight.reshape(width, tp, cols), 1, 0)
         else:
             out_w = out_weight
-        any_spec = pl.BlockSpec(memory_space=pl.ANY)
+        kept = jax.ShapeDtypeStruct if cols % 128 else pltpu.VMEM
+        any_spec = pl.BlockSpec(memory_space=pltpu.HBM)
         vmem_spec = pl.BlockSpec(memory_space=pltpu.VMEM)
         dma = pltpu.SemaphoreType.DMA
-        mixed = pl.pallas_call(
+        flat_rows = rows * heads
+        mixed, committed = pl.pallas_call(
             functools.partial(layer_kernel, kv, tp, proposals, heads, model_width),
-            out_shape=jax.ShapeDtypeStruct((tokens.shape[0], cols), BF16),
-            in_specs=[any_spec, vmem_spec] + [any_spec] * 4 + [vmem_spec] * 2
-            + [pl.BlockSpec(memory_space=pltpu.SMEM), vmem_spec, any_spec, vmem_spec, any_spec],
-            out_specs=vmem_spec,
+            out_shape=(
+                kept((tokens.shape[0], cols), BF16),
+                kept(saved_state.shape, F32),
+            ),
+            in_specs=[any_spec] * 18,
+            out_specs=(vmem_spec, vmem_spec),
             scratch_shapes=[
+                pltpu.VMEM(tokens.shape, BF16),
                 pltpu.VMEM((kv, rows, chunk), BF16),
                 pltpu.VMEM((4, kv, chunk, width), BF16),
-                pltpu.VMEM((heads, seqs, size, size), F32),
+                pltpu.VMEM((heads, seqs, size, size), BF16),
                 pltpu.VMEM((tp, width, cols), BF16),
                 pltpu.VMEM((4, rows, width), F32),
-                pltpu.VMEM((rows, heads * tp), F32),
-                pltpu.VMEM((rows, heads * tp), F32),
+                pltpu.VMEM((rows, 2 * heads * tp), F32),
                 pltpu.VMEM((heads, rows, size), BF16),
                 pltpu.VMEM((2, kv, heads, rows, size), BF16),
                 pltpu.VMEM((kv, rows, cols), F32),
@@ -490,19 +524,33 @@
                 pltpu.VMEM((kv, tp, rows, cols), BF16),
                 pltpu.VMEM((kv, rows), F32),
                 pltpu.VMEM((kv * tp, kv, rows), F32),
-                dma((4, kv)), dma((heads,)), dma((tp,)), dma, dma((kv,)), dma((kv,)),
+                pltpu.VMEM((1, model_width), F32),
+                pltpu.VMEM((heads * tp, model_width), BF16),
+                pltpu.VMEM((heads * tp, model_width), BF16),
+                pltpu.VMEM((1, heads), F32),
+                pltpu.VMEM((1, size), F32),
+                pltpu.VMEM((1, cols), F32),
+                pltpu.VMEM((flat_rows, size), BF16),
+                pltpu.VMEM((flat_rows, size), BF16),
+                pltpu.VMEM((proposals, heads, seqs), F32),
+                pltpu.VMEM((proposals, heads, seqs), F32),
+                pltpu.VMEM((1, seqs), jnp.int32),
+                dma((4, kv)), dma((flat_rows // min(128, flat_rows),)), dma((tp,)), dma, dma((11,)),
+                dma((kv,)), dma((kv,)),
                 dma((kv, tp)), dma((kv, tp)), dma((2, kv, heads)), dma((2, kv, heads)),
                 dma((kv, tp)), dma((kv, tp)), dma((kv * tp,)), dma((kv * tp,)),
             ],
             compiler_params=pltpu.CompilerParams(
-                collective_id=0, has_side_effects=True, vmem_limit_bytes=VMEM_BYTES
+                collective_id=0, has_side_effects=True, vmem_limit_bytes=VMEM_BYTES * 5 // 3 if cols % 128 else VMEM_BYTES
             ),
             name="layer",
-        )(
+        )(*[pltpu.with_memory_space_constraint(x, pltpu.HBM) for x in (
             tokens, pre_gain.reshape(1, model_width), query_weight, key_weight, value_weight,
-            gate_weight, beta_weight.T, decay_weight.T, decay_log, head_gain.reshape(1, size), out_w,
-            post_gain.reshape(1, cols), committed,
-        )
+            gate_weight, beta_weight.T, decay_weight.T, decay_log.reshape(1, heads), head_gain.reshape(1, size), out_w,
+            post_gain.reshape(1, cols), saved_state, earlier_keys.reshape(flat_rows, size),
+            earlier_values.reshape(flat_rows, size), jnp.transpose(earlier_rates, (1, 2, 0)),
+            jnp.transpose(earlier_decays, (1, 2, 0)), accepted.reshape(1, seqs),
+        )])
         return (mixed, committed)
 
     return local

time: 52.3 us -> 47.7 us (0.912)
  Pallas kernels: 48 us -> 42.8 us
  local copies, waits for them, and re-layouts: 3.36 us -> 4.1 us
    pallas_call x1 -> x0, Pallas kernels: 9.46 us -> none  [local(): pl.pallas_call(functools.partial(commit_kernel, proposals), grid=(heads,)...]
    pallas_call x1, Pallas kernels: 38.6 us -> 42.8 us  [local(): pl.pallas_call(functools.partial(layer_kernel, kv, tp, proposals, heads,...]
    unnamed x1 -> x2, local copies, waits for them, and re-layouts: 1.67 us -> 4.1 us
    reshape x1 -> x0, local copies, waits for them, and re-layouts: 1.69 us -> none  [local(): earlier_values.reshape(rows, width)]
where the time goes in v1:
time: 47.7 us; the launch traced here: 47.6 us
  Pallas kernels  42.8 us (90%)
  local copies, waits for them, and re-layouts  4.1 us (9%)
  between operations  0.65 us (1%)
    pallas_call x1, Pallas kernels, local(): pl.pallas_call(functools.partial(layer_kernel, kv, tp, proposals, heads,...  42.8 us
    unnamed x2, local copies, waits for them, and re-layouts  4.1 us

profile of v1, /device:TPU:0, one launch (start us, length us, event | category | flops | bytes accessed | tf_op | source)
XLA Modules:
  0.0 47.6 jit_solution(17180029401237893298)
XLA Ops:
  0.6 42.8 %layer.1 = (bf16[512,256]{1,0:T(8,128)(2,1)S(1)}, f32[32,4,128,128]{3,2,1,0:T(8,128)S(1)}) custom-call(bf16[512,512]{1,0:T(8,128)(2,1)} %tokens.1, f32[1,2048]{1,0:T(1,128)} %bitcast.15, bf16[2048,512]{1,0:T(8,128)(2,1)} %qw.1, bf16[2048,512]{1,0:T(8,128)(2,1)} %kw.1, bf16[2048,512]{1,0:T(8,128)(2,1)} %vw.1, bf16[2048,512]{1,0:T(8,128)(2,1)} %gw.1, ...), custom_call_target="tpu_custom_call" | custom-call | tf_op jit(solution)/shard_map/layer/pallas_call | solution.py:504
  43.5 0.7 %copy.22 = bf16[512,256]{1,0:T(8,128)(2,1)} copy(bf16[512,256]{1,0:T(8,128)(2,1)S(1)} %get-tuple-element.2) | data formatting | bytes 524288
  44.2 3.4 %copy.23 = f32[32,4,128,128]{3,2,1,0:T(8,128)} copy(f32[32,4,128,128]{3,2,1,0:T(8,128)S(1)} %get-tuple-element.3) | data formatting | bytes 16777216

commit v2 on v1

--- a/solution.py
+++ b/solution.py
@@ -167,11 +167,16 @@
     cols = out.shape[1]
     weights = (qw, kw, vw, gw)
 
-    def source(d):
-        return lax.rem(me - d + kv, kv)
-
-    def target(d):
-        return lax.rem(me + d, kv)
+    more_left = lax.div(2 * me, kv)
+    both = more_left * (kv - 1 - me) + (1 - more_left) * me
+
+    def nearest(j):
+        if j == 0:
+            return me
+        paired = lax.div(2 * both - j + kv, kv)
+        turned = me - (j + 1) // 2 if j % 2 else me + j // 2
+        beyond = me + (1 - 2 * more_left) * (j - both)
+        return paired * turned + (1 - paired) * beyond
 
     barrier = pltpu.get_barrier_semaphore()
     group = kv * tp
@@ -195,6 +200,7 @@
     for i, (src, dst) in enumerate(pairs_small):
         local["small", i] = pltpu.make_async_copy(src, dst, small_sem.at[i])
         local["small", i].start()
+    local["tok"].wait()
     block_rows = min(128, ekeys.shape[0])
     blocks_n = ekeys.shape[0] // block_rows
     block_seqs = state.shape[0] // blocks_n
@@ -202,12 +208,15 @@
         span = pl.ds(b * block_seqs, block_seqs)
         local["s", b] = pltpu.make_async_copy(state.at[span], com.at[span], s_sem.at[b])
         local["s", b].start()
-    for d in range(kv):
+
+    def fetch_weights(d):
+        c = nearest(d)
         for i in range(4):
             local["w", i, d] = pltpu.make_async_copy(
-                weights[i].at[pl.ds(source(d) * chunk, chunk), :], wv.at[i, d], w_sem.at[i, d]
+                weights[i].at[pl.ds(c * chunk, chunk), :], wv.at[i, d], w_sem.at[i, d]
             )
             local["w", i, d].start()
+
     for o in range(tp):
         half = lax.rem(core + o, tp)
         if len(ow.shape) == 3:
@@ -217,32 +226,44 @@
         local["o", o] = pltpu.make_async_copy(src, owv.at[o], ow_sem.at[o])
         local["o", o].start()
 
-    local["tok"].wait()
     pl.semaphore_wait(barrier, group - 1)
 
     part_rows = rows // tp
     mine_rows = pl.ds(pl.multiple_of(core * part_rows, part_rows), part_rows)
     sent = {}
     halves = {}
-    for d in range(1, kv):
+    for d in range(kv - 1, 0, -1):
+        c = nearest(d)
         sent[d] = pltpu.make_async_remote_copy(
             src_ref=tokv.at[
-                pl.ds(pl.multiple_of(target(d) * rows + core * part_rows, part_rows), part_rows), :
+                pl.ds(pl.multiple_of(c * rows + core * part_rows, part_rows), part_rows), :
             ],
-            dst_ref=tok.at[d, mine_rows],
-            send_sem=tok_send.at[d],
-            recv_sem=tok_recv.at[d],
-            device_id={"kv": target(d)},
+            dst_ref=tok.at[me, mine_rows],
+            send_sem=tok_send.at[c],
+            recv_sem=tok_recv.at[me],
+            device_id={"kv": c},
             device_id_type=MESH_IDS,
         )
         sent[d].start()
 
+    def arrival(d):
+        c = nearest(d)
+        return pltpu.make_async_remote_copy(
+            src_ref=tok.at[c, mine_rows],
+            dst_ref=tok.at[c, mine_rows],
+            send_sem=tok_send.at[c],
+            recv_sem=tok_recv.at[c],
+            device_id={"kv": c},
+            device_id_type=MESH_IDS,
+        )
+
     def hand_over(d):
-        sent[d].wait_recv()
+        c = nearest(d)
+        arrival(d).wait_recv()
         for o in range(1, tp):
             halves[d, o] = pltpu.make_async_remote_copy(
-                src_ref=tok.at[d, mine_rows],
-                dst_ref=tok.at[d, mine_rows],
+                src_ref=tok.at[c, mine_rows],
+                dst_ref=tok.at[c, mine_rows],
                 send_sem=half_send.at[d, o],
                 recv_sem=half_recv.at[d, o],
                 device_id={"tp": lax.rem(core + o, tp)},
@@ -254,12 +275,12 @@
         if d > 0:
             for o in range(1, tp):
                 halves[d, o].wait_recv()
-        c = source(d)
+        c = nearest(d)
         span = pl.ds(pl.multiple_of(c * chunk, 128), chunk)
         if d == 0:
             wide = tokv[pl.ds(pl.multiple_of(me * rows, rows), rows), :].astype(F32)
         else:
-            wide = tok[d].astype(F32)
+            wide = tok[c].astype(F32)
         scaled = (wide * gains[:, span]).astype(BF16)
         thin = mm_nt(scaled, jnp.concatenate([beta_t[:, span], decay_t[:, span]], axis=0))
         if d == 0:
@@ -280,19 +301,21 @@
     table = commit_table(proposals, heads, erates[...], edecays[...], accepted[...])
     commit_masks = head_masks(block_rows, proposals * heads, heads)
     squares = jnp.zeros((rows, 1), F32)
-    steps = max(blocks_n, kv)
-    for b in range(steps):
-        if b < blocks_n:
-            span = slice(b * block_rows, (b + 1) * block_rows)
-            local["s", b].wait()
-            commit_block(
-                b, proposals, heads, table, ekeys[span], evalues[span], commit_masks, com, sbf
-            )
-        if 1 <= b < kv:
-            hand_over(b)
-        if b >= 1 and b - 1 < kv - 1:
-            squares = project(b - 1, squares)
-    squares = project(kv - 1, squares)
+    for b in range(blocks_n):
+        span = slice(b * block_rows, (b + 1) * block_rows)
+        local["s", b].wait()
+        for d in range(b * kv // blocks_n, (b + 1) * kv // blocks_n):
+            fetch_weights(d)
+        commit_block(
+            b, proposals, heads, table, ekeys[span], evalues[span], commit_masks, com, sbf
+        )
+    squares = project(0, squares)
+    for d in range(1, kv):
+        hand_over(d)
+        if d > 1:
+            squares = project(d - 1, squares)
+    if kv > 1:
+        squares = project(kv - 1, squares)
     inverse = lax.rsqrt(squares / model_width + EPS)
 
     same, incl, strict = masks_of(rows, proposals)
@@ -317,13 +340,18 @@
         step *= 2
     cum_t = cum.T
 
+    def parent(s):
+        return s - 1 if s % 2 else s - 2
+
     def hop(way, s, h):
-        step = 1 if way == 0 else kv - 1
+        step = s - parent(s)
+        if way:
+            step = kv - step
         return pltpu.make_async_remote_copy(
-            src_ref=att.at[h] if s == 0 else passed.at[way, s, h],
-            dst_ref=passed.at[way, s + 1, h],
+            src_ref=att.at[h] if parent(s) == 0 else passed.at[way, parent(s), h],
+            dst_ref=passed.at[way, s, h],
             send_sem=att_send.at[way, s, h],
-            recv_sem=att_recv.at[way, s + 1, h],
+            recv_sem=att_recv.at[way, s, h],
             device_id={"kv": lax.rem(me + step, kv)},
             device_id_type=MESH_IDS,
         )
@@ -331,35 +359,52 @@
     def arrives(way, s):
         return me - s >= 0 if way == 0 else me + s < kv
 
-    def leaves(way):
-        return me + 1 < kv if way == 0 else me >= 1
+    def leaves(way, reach):
+        return me + reach < kv if way == 0 else me >= reach
+
+    def children(s):
+        return [t for t in (s + 2, s + 1) if t < kv]
+
+    lag = 3
+
+    def relays(s):
+        return s % 2 == 0 and bool(children(s))
 
     def advance(turn):
-        for s in range(kv):
-            h = turn - s
-            if not 0 <= h < heads:
+        for s in range(0, kv, 2):
+            h = turn - lag * (s // 2)
+            if not 0 <= h < heads or not relays(s):
                 continue
             for way in range(2):
-                if s == 0:
-                    @pl.when(leaves(way))
+                if s > 0:
+                    @pl.when(arrives(way, s) & leaves(way, 1))
                     def _():
-                        hop(way, 0, h).start()
-                else:
-                    @pl.when(arrives(way, s))
+                        hop(way, s, h).wait_recv()
+                for t in children(s):
+                    @pl.when(arrives(way, s) & leaves(way, t - s))
                     def _():
-                        hop(way, s - 1, h).wait_recv()
-                    if s < kv - 1:
-                        @pl.when(arrives(way, s) & leaves(way))
-                        def _():
-                            hop(way, s, h).start()
+                        hop(way, t, h).start()
+
+    def gather(way, s):
+        if way is None:
+            return
+        here = arrives(way, s)
+        if relays(s):
+            here = here & jnp.logical_not(leaves(way, 1))
+
+        @pl.when(here)
+        def _():
+            for h in range(heads):
+                hop(way, s, h).wait_recv()
 
     def settle():
-        for s in range(kv - 1):
-            for way in range(2):
-                @pl.when(arrives(way, s) & leaves(way))
-                def _():
-                    for h in range(heads):
-                        hop(way, s, h).wait_send()
+        for s in range(0, kv, 2):
+            for t in children(s):
+                for way in range(2):
+                    @pl.when(arrives(way, s) & leaves(way, t - s))
+                    def _():
+                        for h in range(heads):
+                            hop(way, t, h).wait_send()
 
     for first in range(heads):
         batch = range(first, first + 1)
@@ -417,34 +462,36 @@
         total = jnp.sum(own * own, axis=1, keepdims=True)
         sums[pl.ds(c, 1), :] = jnp.broadcast_to(total, (rows, rows)).T[0:1]
 
-    def blocks(turn):
-        if turn < heads:
+    def blocks(s):
+        if s == 0:
             return [(True, me, None)]
-        s = turn - heads + 1
         return [(arrives(way, s), me - s if way == 0 else me + s, way) for way in range(2)]
 
-    combine(me, [att[h] for h in range(heads)])
-    for turn in range(heads, heads + kv - 1):
+    def finish_at(s):
+        if s == 0:
+            finish(me)
+            return
+        for here, c, way in blocks(s):
+            @pl.when(here)
+            def _():
+                finish(c)
+
+    deepest = max([s for s in range(kv) if relays(s)], default=0)
+    for turn in range(heads, heads + lag * (deepest // 2)):
         advance(turn)
-        s = turn - heads + 1
-        for here, c, way in blocks(turn):
+        if turn == heads:
+            combine(me, [att[h] for h in range(heads)])
+    if not deepest:
+        combine(me, [att[h] for h in range(heads)])
+    for s in range(1, kv):
+        for here, c, way in blocks(s):
+            gather(way, s)
+
             @pl.when(here)
             def _():
                 combine(c, [passed[way, s, h] for h in range(heads)])
-        if s == 1:
-            finish(me)
-        else:
-            for here, c, way in blocks(turn - 1):
-                @pl.when(here)
-                def _():
-                    finish(c)
-    if kv > 1:
-        for here, c, way in blocks(heads + kv - 2):
-            @pl.when(here)
-            def _():
-                finish(c)
-    else:
-        finish(me)
+        finish_at(s - 1)
+    finish_at(kv - 1)
     tells = {}
     for o in range(1, group):
         tells[o] = pltpu.make_async_remote_copy(
@@ -456,6 +503,13 @@
             device_id_type=MESH_IDS,
         )
         tells[o].start()
+    totals = sums[...]
+    for o in range(1, group):
+        tells[o].wait_recv()
+        totals = totals + sumall[o]
+    sums_factor = lax.rsqrt(totals / model_width + EPS)
+    for o in range(1, group):
+        tells[o].wait_send()
     settle()
     for d in range(1, kv):
         sent[d].wait_send()
@@ -464,13 +518,6 @@
     for c in range(kv):
         for o in range(1, tp):
             swap(c, o).wait_send()
-    totals = sums[...]
-    for o in range(1, group):
-        tells[o].wait_recv()
-        totals = totals + sumall[o]
-    sums_factor = lax.rsqrt(totals / model_width + EPS)
-    for o in range(1, group):
-        tells[o].wait_send()
     for c in range(kv):
         factor = jnp.broadcast_to(sums_factor[c:c + 1, :], (rows, rows)).T[:, 0:1]
         out[c * rows:(c + 1) * rows, :] = (part[c] * factor * post[...]).astype(BF16)

time: 47.7 us -> 38.5 us (0.81)
  Pallas kernels: 42.8 us -> 33.6 us
    pallas_call x1, Pallas kernels: 42.8 us -> 33.6 us  [local(): pl.pallas_call(functools.partial(layer_kernel, kv, tp, proposals, heads,...]
where the time goes in v2:
time: 38.5 us; the launch traced here: 38.3 us
  Pallas kernels  33.6 us (87%)
  local copies, waits for them, and re-layouts  4.1 us (11%)
  between operations  0.65 us (2%)
    pallas_call x1, Pallas kernels, local(): pl.pallas_call(functools.partial(layer_kernel, kv, tp, proposals, heads,...  33.6 us
    unnamed x2, local copies, waits for them, and re-layouts  4.1 us

profile of v2, /device:TPU:0, one launch (start us, length us, event | category | flops | bytes accessed | tf_op | source)
XLA Modules:
  0.0 38.3 jit_solution(836573278259134354)
XLA Ops:
  0.6 33.6 %layer.1 = (bf16[512,256]{1,0:T(8,128)(2,1)S(1)}, f32[32,4,128,128]{3,2,1,0:T(8,128)S(1)}) custom-call(bf16[512,512]{1,0:T(8,128)(2,1)} %tokens.1, f32[1,2048]{1,0:T(1,128)} %bitcast.15, bf16[2048,512]{1,0:T(8,128)(2,1)} %qw.1, bf16[2048,512]{1,0:T(8,128)(2,1)} %kw.1, bf16[2048,512]{1,0:T(8,128)(2,1)} %vw.1, bf16[2048,512]{1,0:T(8,128)(2,1)} %gw.1, ...), custom_call_target="tpu_custom_call" | custom-call | tf_op jit(solution)/shard_map/layer/pallas_call | solution.py:551
  34.2 0.7 %copy.22 = bf16[512,256]{1,0:T(8,128)(2,1)} copy(bf16[512,256]{1,0:T(8,128)(2,1)S(1)} %get-tuple-element.2) | data formatting | bytes 524288
  34.9 3.4 %copy.23 = f32[32,4,128,128]{3,2,1,0:T(8,128)} copy(f32[32,4,128,128]{3,2,1,0:T(8,128)S(1)} %get-tuple-element.3) | data formatting | bytes 16777216

commit v3 on v2

--- a/solution.py
+++ b/solution.py
@@ -1,4 +1,5 @@
 import functools
+import math
 
 import jax
 import jax.numpy as jnp
@@ -154,8 +155,8 @@
     kv, tp, proposals, heads, model_width,
     tokens, gains_h, qw, kw, vw, gw, beta_h, decay_h, log_h, head_gain_h, ow, post_h, state,
     ekeys_h, evalues_h, erates_h, edecays_h, accepted_h,
-    out, com,
-    tokv, tok, wv, sbf, owv, acc, sacc, att, passed, part, give, take, sums, sumall,
+    part, factors, com,
+    tokv, tok, wv, sbf, owv, acc, sacc, att, passed, give, take, sums, sumall,
     gains, beta_t, decay_t, log_rate, head_gain, post, ekeys, evalues, erates, edecays, accepted,
     w_sem, s_sem, ow_sem, own_sem, small_sem, tok_send, tok_recv, half_send, half_recv,
     att_send, att_recv, tp_send, tp_recv, sum_send, sum_recv,
@@ -164,17 +165,15 @@
     core = lax.axis_index("tp")
     rows, chunk = tok.shape[1], tok.shape[2]
     size = head_gain.shape[1]
-    cols = out.shape[1]
+    cols = part.shape[2]
     weights = (qw, kw, vw, gw)
 
     more_left = lax.div(2 * me, kv)
     both = more_left * (kv - 1 - me) + (1 - more_left) * me
 
     def nearest(j):
-        if j == 0:
-            return me
         paired = lax.div(2 * both - j + kv, kv)
-        turned = me - (j + 1) // 2 if j % 2 else me + j // 2
+        turned = me + (1 - 2 * (j % 2)) * ((j + 1) // 2)
         beyond = me + (1 - 2 * more_left) * (j - both)
         return paired * turned + (1 - paired) * beyond
 
@@ -232,7 +231,7 @@
     mine_rows = pl.ds(pl.multiple_of(core * part_rows, part_rows), part_rows)
     sent = {}
     halves = {}
-    for d in range(kv - 1, 0, -1):
+    for d in range(1, kv):
         c = nearest(d)
         sent[d] = pltpu.make_async_remote_copy(
             src_ref=tokv.at[
@@ -309,13 +308,10 @@
         commit_block(
             b, proposals, heads, table, ekeys[span], evalues[span], commit_masks, com, sbf
         )
-    squares = project(0, squares)
     for d in range(1, kv):
         hand_over(d)
-        if d > 1:
-            squares = project(d - 1, squares)
-    if kv > 1:
-        squares = project(kv - 1, squares)
+        squares = project(d - 1, squares)
+    squares = project(kv - 1, squares)
     inverse = lax.rsqrt(squares / model_width + EPS)
 
     same, incl, strict = masks_of(rows, proposals)
@@ -340,8 +336,10 @@
         step *= 2
     cum_t = cum.T
 
+    stride = 2
+
     def parent(s):
-        return s - 1 if s % 2 else s - 2
+        return (s - 1) // stride * stride
 
     def hop(way, s, h):
         step = s - parent(s)
@@ -363,16 +361,16 @@
         return me + reach < kv if way == 0 else me >= reach
 
     def children(s):
-        return [t for t in (s + 2, s + 1) if t < kv]
+        return [t for t in range(s + stride, s, -1) if t < kv]
 
     lag = 3
 
     def relays(s):
-        return s % 2 == 0 and bool(children(s))
+        return s % stride == 0 and bool(children(s))
 
     def advance(turn):
-        for s in range(0, kv, 2):
-            h = turn - lag * (s // 2)
+        for s in range(0, kv, stride):
+            h = turn - lag * (s // stride)
             if not 0 <= h < heads or not relays(s):
                 continue
             for way in range(2):
@@ -398,7 +396,7 @@
                 hop(way, s, h).wait_recv()
 
     def settle():
-        for s in range(0, kv, 2):
+        for s in range(0, kv, stride):
             for t in children(s):
                 for way in range(2):
                     @pl.when(arrives(way, s) & leaves(way, t - s))
@@ -458,7 +456,7 @@
         for o in range(1, tp):
             swap(c, o).wait_recv()
             own = own + take[c, o].astype(F32)
-        part[c] = own
+        part[c] = own * post[...]
         total = jnp.sum(own * own, axis=1, keepdims=True)
         sums[pl.ds(c, 1), :] = jnp.broadcast_to(total, (rows, rows)).T[0:1]
 
@@ -477,7 +475,7 @@
                 finish(c)
 
     deepest = max([s for s in range(kv) if relays(s)], default=0)
-    for turn in range(heads, heads + lag * (deepest // 2)):
+    for turn in range(heads, heads + lag * (deepest // stride)):
         advance(turn)
         if turn == heads:
             combine(me, [att[h] for h in range(heads)])
@@ -507,7 +505,7 @@
     for o in range(1, group):
         tells[o].wait_recv()
         totals = totals + sumall[o]
-    sums_factor = lax.rsqrt(totals / model_width + EPS)
+    factors[...] = lax.rsqrt(totals / model_width + EPS)
     for o in range(1, group):
         tells[o].wait_send()
     settle()
@@ -518,9 +516,28 @@
     for c in range(kv):
         for o in range(1, tp):
             swap(c, o).wait_send()
+
+
+def scale_rows(part, factors, mixed):
+    kv, rows, cols = part.shape
     for c in range(kv):
-        factor = jnp.broadcast_to(sums_factor[c:c + 1, :], (rows, rows)).T[:, 0:1]
-        out[c * rows:(c + 1) * rows, :] = (part[c] * factor * post[...]).astype(BF16)
+        factor = jnp.broadcast_to(factors[c:c + 1, :], (rows, rows)).T[:, 0:1]
+        mixed[c * rows:(c + 1) * rows, :] = (part[c] * factor).astype(BF16)
+
+
+def store_kernel(pieces, part, factors, com, mixed_out, com_out, mixed, sems):
+    copies = []
+    size = com.shape[0] // pieces
+    for i in range(pieces):
+        span = pl.ds(i * size, size)
+        copies.append(pltpu.make_async_copy(com.at[span], com_out.at[span], sems.at[i]))
+    for copy in copies:
+        copy.start()
+    scale_rows(part, factors, mixed)
+    copies.append(pltpu.make_async_copy(mixed, mixed_out, sems.at[pieces]))
+    copies[-1].start()
+    for copy in copies:
+        copy.wait()
 
 
 def make_local(mesh):
@@ -548,14 +565,15 @@
         vmem_spec = pl.BlockSpec(memory_space=pltpu.VMEM)
         dma = pltpu.SemaphoreType.DMA
         flat_rows = rows * heads
-        mixed, committed = pl.pallas_call(
+        part, factors, committed = pl.pallas_call(
             functools.partial(layer_kernel, kv, tp, proposals, heads, model_width),
             out_shape=(
-                kept((tokens.shape[0], cols), BF16),
+                kept((kv, rows, cols), F32),
+                kept((kv, rows), F32),
                 kept(saved_state.shape, F32),
             ),
             in_specs=[any_spec] * 18,
-            out_specs=(vmem_spec, vmem_spec),
+            out_specs=(vmem_spec,) * 3,
             scratch_shapes=[
                 pltpu.VMEM(tokens.shape, BF16),
                 pltpu.VMEM((kv, rows, chunk), BF16),
@@ -566,7 +584,6 @@
                 pltpu.VMEM((rows, 2 * heads * tp), F32),
                 pltpu.VMEM((heads, rows, size), BF16),
                 pltpu.VMEM((2, kv, heads, rows, size), BF16),
-                pltpu.VMEM((kv, rows, cols), F32),
                 pltpu.VMEM((kv, tp, rows, cols), BF16),
                 pltpu.VMEM((kv, tp, rows, cols), BF16),
                 pltpu.VMEM((kv, rows), F32),
@@ -598,7 +615,25 @@
             earlier_values.reshape(flat_rows, size), jnp.transpose(earlier_rates, (1, 2, 0)),
             jnp.transpose(earlier_decays, (1, 2, 0)), accepted.reshape(1, seqs),
         )])
-        return (mixed, committed)
+        pieces = math.gcd(seqs, 8)
+        mixed_shape = (tokens.shape[0], cols)
+        if cols % 128:
+            mixed = pl.pallas_call(
+                scale_rows, out_shape=jax.ShapeDtypeStruct(mixed_shape, BF16), name="scale"
+            )(part, factors)
+            return (mixed, committed)
+        return pl.pallas_call(
+            functools.partial(store_kernel, pieces),
+            out_shape=(
+                jax.ShapeDtypeStruct(mixed_shape, BF16),
+                jax.ShapeDtypeStruct(committed.shape, F32),
+            ),
+            in_specs=[vmem_spec] * 3,
+            out_specs=(any_spec, any_spec),
+            scratch_shapes=[pltpu.VMEM(mixed_shape, BF16), dma((pieces + 1,))],
+            compiler_params=pltpu.CompilerParams(vmem_limit_bytes=VMEM_BYTES // 4),
+            name="store",
+        )(*[pltpu.with_memory_space_constraint(x, pltpu.VMEM) for x in (part, factors, committed)])
 
     return local
 

time: 38.5 us -> 36.7 us (0.953)
  local copies, waits for them, and re-layouts: 4.1 us -> 0 us
  Pallas kernels: 33.6 us -> 35.9 us
    unnamed x2 -> x0, local copies, waits for them, and re-layouts: 4.1 us -> none
    pallas_call x0 -> x1, Pallas kernels: none -> 3.43 us  [local(): pl.pallas_call(functools.partial(store_kernel, pieces), out_shape=(jax.Sh...]
    pallas_call x1, Pallas kernels: 33.6 us -> 32.4 us  [local(): pl.pallas_call(functools.partial(layer_kernel, kv, tp, proposals, heads,...]
where the time goes in v3:
time: 36.7 us; the launch traced here: 36.5 us
  Pallas kernels  35.9 us (98%)
  between operations  0.65 us (2%)
    pallas_call x1, Pallas kernels, local(): pl.pallas_call(functools.partial(layer_kernel, kv, tp, proposals, heads,...  32.4 us
    pallas_call x1, Pallas kernels, local(): pl.pallas_call(functools.partial(store_kernel, pieces), out_shape=(jax.Sh...  3.43 us

profile of v3, /device:TPU:0, one launch (start us, length us, event | category | flops | bytes accessed | tf_op | source)
XLA Modules:
  0.0 36.5 jit_solution(14734210481459978144)
XLA Ops:
  0.6 32.4 %layer.1 = (f32[4,128,256]{2,1,0:T(8,128)S(1)}, f32[4,128]{1,0:T(4,128)S(1)}, f32[32,4,128,128]{3,2,1,0:T(8,128)S(1)}) custom-call(bf16[512,512]{1,0:T(8,128)(2,1)} %tokens.1, f32[1,2048]{1,0:T(1,128)} %bitcast.15, bf16[2048,512]{1,0:T(8,128)(2,1)} %qw.1, bf16[2048,512]{1,0:T(8,128)(2,1)} %kw.1, bf16[2048,512]{1,0:T(8,128)(2,1)} %vw.1, ...), custom_call_target="tpu_custom_call" | custom-call | tf_op jit(solution)/shard_map/layer/pallas_call | solution.py:568
  33.1 3.4 %store.1 = (bf16[512,256]{1,0:T(8,128)(2,1)}, f32[32,4,128,128]{3,2,1,0:T(8,128)}) custom-call(f32[4,128,256]{2,1,0:T(8,128)S(1)} %get-tuple-element.5.part, f32[4,128]{1,0:T(4,128)S(1)} %get-tuple-element.6.factors, f32[32,4,128,128]{3,2,1,0:T(8,128)S(1)} %get-tuple-element.7.com), custom_call_target="tpu_custom_call" | custom-call | tf_op jit(solution)/shard_map/store/pallas_call | solution.py:625

commit v4 on v3

--- a/solution.py
+++ b/solution.py
@@ -308,10 +308,13 @@
         commit_block(
             b, proposals, heads, table, ekeys[span], evalues[span], commit_masks, com, sbf
         )
+    for d in range(1, min(2, kv)):
+        hand_over(d)
+    squares = project(0, squares)
+    for d in range(2, kv):
+        hand_over(d)
     for d in range(1, kv):
-        hand_over(d)
-        squares = project(d - 1, squares)
-    squares = project(kv - 1, squares)
+        squares = project(d, squares)
     inverse = lax.rsqrt(squares / model_width + EPS)
 
     same, incl, strict = masks_of(rows, proposals)
@@ -368,6 +371,9 @@
     def relays(s):
         return s % stride == 0 and bool(children(s))
 
+    def at_end(way, reach):
+        return me + reach == kv - 1 if way == 0 else me == reach
+
     def advance(turn):
         for s in range(0, kv, stride):
             h = turn - lag * (s // stride)
@@ -379,9 +385,19 @@
                     def _():
                         hop(way, s, h).wait_recv()
                 for t in children(s):
-                    @pl.when(arrives(way, s) & leaves(way, t - s))
+                    goes = arrives(way, s) & leaves(way, t - s)
+                    if t == 1:
+                        goes = goes & at_end(way, 1)
+
+                    @pl.when(goes)
                     def _():
                         hop(way, t, h).start()
+        if turn == heads:
+            for way in range(2):
+                @pl.when(leaves(way, 1) & jnp.logical_not(at_end(way, 1)))
+                def _():
+                    for h in range(heads):
+                        hop(way, 1, h).start()
 
     def gather(way, s):
         if way is None:

time: 36.7 us -> 36.3 us (0.989)
  Pallas kernels: 35.9 us -> 35.5 us
where the time goes in v4:
time: 36.3 us; the launch traced here: 36.2 us
  Pallas kernels  35.5 us (98%)
  between operations  0.65 us (2%)
    pallas_call x1, Pallas kernels, local(): pl.pallas_call(functools.partial(layer_kernel, kv, tp, proposals, heads,...  32.1 us
    pallas_call x1, Pallas kernels, local(): pl.pallas_call(functools.partial(store_kernel, pieces), out_shape=(jax.Sh...  3.43 us

profile of v4, /device:TPU:0, one launch (start us, length us, event | category | flops | bytes accessed | tf_op | source)
XLA Modules:
  0.0 36.2 jit_solution(13924139035001472176)
XLA Ops:
  0.6 32.1 %layer.1 = (f32[4,128,256]{2,1,0:T(8,128)S(1)}, f32[4,128]{1,0:T(4,128)S(1)}, f32[32,4,128,128]{3,2,1,0:T(8,128)S(1)}) custom-call(bf16[512,512]{1,0:T(8,128)(2,1)} %tokens.1, f32[1,2048]{1,0:T(1,128)} %bitcast.15, bf16[2048,512]{1,0:T(8,128)(2,1)} %qw.1, bf16[2048,512]{1,0:T(8,128)(2,1)} %kw.1, bf16[2048,512]{1,0:T(8,128)(2,1)} %vw.1, ...), custom_call_target="tpu_custom_call" | custom-call | tf_op jit(solution)/shard_map/layer/pallas_call | solution.py:584
  32.8 3.4 %store.1 = (bf16[512,256]{1,0:T(8,128)(2,1)}, f32[32,4,128,128]{3,2,1,0:T(8,128)}) custom-call(f32[4,128,256]{2,1,0:T(8,128)S(1)} %get-tuple-element.5.part, f32[4,128]{1,0:T(4,128)S(1)} %get-tuple-element.6.factors, f32[32,4,128,128]{3,2,1,0:T(8,128)S(1)} %get-tuple-element.7.com), custom_call_target="tpu_custom_call" | custom-call | tf_op jit(solution)/shard_map/store/pallas_call | solution.py:641
